TPU v7x, 32 devices: a whole 2x2x4 slice. The times are simulated.
32 devices in a mesh: sp: 16 (over z, y, x), tp: 2 (over core).
Axes of the slice: x: 2, y: 2, z: 4, core: 2. Of those that a mesh axis runs over, the one named last changes fastest.
Arguments:
- residual: bfloat16 [4096, 2048], P(('sp', 'tp')), may hold values from -6 to 6
- query_rows: bfloat16 [4096, 1024], P('sp', 'tp'), may hold values from -141 to 141
- key_rows: bfloat16 [4096, 1024], P('sp', 'tp'), may hold values from -7.8 to 7.8
- value_rows: bfloat16 [4096, 1024], P('sp', 'tp'), may hold values from -6 to 6
- mix_lambda: float32 [8], P('tp'), may hold values from 0.3 to 0.8
- documents: int32 [4096], P('sp'), may hold values from 0 to 7, never falling along the last dimension, each value on 1 to 768 neighbouring positions
- out_weight: bfloat16 [1024, 2048], replicated, may hold values from -0.1875 to 0.1875
- norm_gain: float32 [2048], replicated, may hold values from 0.1 to 1.9
- gate_weight: bfloat16 [16, 2048, 2048], P('sp', None, 'tp'), may hold values from -0.125 to 0.125
- up_weight: bfloat16 [16, 2048, 2048], P('sp', None, 'tp'), may hold values from -0.125 to 0.125
- down_weight: bfloat16 [16, 2048, 2048], P('sp', 'tp'), may hold values from -0.125 to 0.125
- routes: int32 [4096, 2], P(('sp', 'tp')), may hold values from 0 to 15, all different within a row; in each aligned block of 128 rows (0 to 127, 128 to 255, ...) at most 32 rows name the same one
- route_weights: float32 [4096, 2], P(('sp', 'tp')), may hold values from 0.25 to 1
Outputs:
- layer_out: bfloat16 [4096, 2048], P(('sp', 'tp'))
Inputs may be any that keep to these rules, and one draw needn't show every extreme that they name: `documents`: document numbers never fall along the sequence; a document covers at most 768 positions, and one covers exactly that many. `routes`: each row names two different experts. Among the rows of one index of sp+tp, no expert is named by more than 32 rows, and in every draw some expert is named by exactly 32 rows of some such block.
All inputs are finite; a program needn't handle non-finite values.
Results may differ from a plain program's by a relative error of at most 0.013.
Values may be sent and summed in bfloat16 or wider, within the bound.
A program may use at most 128 MiB of HBM per device.

v0:
```python
import functools

import jax
import jax.numpy as jnp
from jax import lax
from jax.experimental import pallas as pl
from jax.experimental.pallas import tpu as pltpu
from jax.sharding import PartitionSpec as P

HD = 64
REACH = 3
MESH = pl.DeviceIdType.MESH
VMEM = pl.BlockSpec(memory_space=pltpu.VMEM)


def offsets_of(reach):
    return [sign * step for step in range(1, reach + 1) for sign in (1, -1)]


def halo_kernel(
    count, k_ref, v_ref, id_ref, k_out, v_out, id_out, send_sem, recv_sem, pass_sem
):
    me, core = lax.axis_index("sp"), lax.axis_index("tp")
    offsets = offsets_of(REACH)
    group = REACH + 1
    barrier = pltpu.get_barrier_semaphore()

    def inside(offset):
        return jnp.logical_and(me + offset >= 0, me + offset < count)

    for offset in offsets_of(group):

        @pl.when(inside(offset))
        def _():
            pl.semaphore_signal(barrier, inc=1, device_id=(me + offset, core), device_id_type=MESH)

    pl.semaphore_wait(barrier, jnp.minimum(me, group) + jnp.minimum(count - 1 - me, group))

    place = me % group

    def near(offset):
        return jnp.logical_and(place + offset >= 0, place + offset < group)

    def opposite(offset):
        return place + (place + offset + group) % group == group - 1

    def copies(at, offset):
        slot = REACH - offset
        return [
            pltpu.make_async_remote_copy(
                src_ref=source,
                dst_ref=target.at[slot],
                send_sem=send_sem.at[at, which],
                recv_sem=recv_sem.at[at, which],
                device_id=(me + offset, core),
                device_id_type=MESH,
            )
            for which, (source, target) in enumerate(
                ((id_ref, id_out), (k_ref, k_out), (v_ref, v_out))
            )
        ]

    def passes(at, offset):
        hop = group if offset < 0 else -group
        beyond = offset + hop
        return [
            pltpu.make_async_remote_copy(
                src_ref=part.at[REACH - offset],
                dst_ref=part.at[REACH - beyond],
                send_sem=pass_sem.at[at, which],
                recv_sem=recv_sem.at[offsets.index(beyond), which],
                device_id=(me + hop, core),
                device_id_type=MESH,
            )
            for which, part in enumerate((id_out, k_out, v_out))
        ]

    def sends(offset):
        return jnp.logical_and(inside(offset), jnp.logical_or(near(offset), opposite(offset)))

    def relays(offset):
        hop = group if offset < 0 else -group
        aligned = jnp.logical_and(inside(-offset), near(-offset))
        aligned = jnp.logical_and(aligned, jnp.logical_not(opposite(-offset)))
        return jnp.logical_and(aligned, inside(hop))

    for at, offset in enumerate(offsets):

        @pl.when(sends(offset))
        def _():
            for copy in copies(at, offset):
                copy.start()

    k_out[REACH] = k_ref[...]
    v_out[REACH] = v_ref[...]
    id_out[REACH] = id_ref[...]
    for offset in offsets:

        @pl.when(jnp.logical_not(inside(-offset)))
        def _():
            slot = REACH - offset
            k_out[slot] = jnp.zeros_like(k_ref)
            v_out[slot] = jnp.zeros_like(v_ref)
            id_out[slot] = jnp.full_like(id_ref, -1)

    for which in range(3):
        for at, offset in enumerate(offsets):

            @pl.when(relays(offset))
            def _():
                copies(at, offset)[which].wait_recv()
                passes(at, offset)[which].start()

    for at, offset in enumerate(offsets):

        @pl.when(jnp.logical_and(inside(-offset), jnp.logical_not(relays(offset))))
        def _():
            for copy in copies(at, offset):
                copy.wait_recv()

    for at, offset in enumerate(offsets):

        @pl.when(sends(offset))
        def _():
            for copy in copies(at, offset):
                copy.wait_send()

        @pl.when(relays(offset))
        def _():
            for copy in passes(at, offset):
                copy.wait_send()


def halo(count, key_rows, value_rows, ids):
    slots = 2 * REACH + 1
    outs = [
        jax.ShapeDtypeStruct((slots,) + part.shape, part.dtype)
        for part in (key_rows, value_rows, ids)
    ]
    return pl.pallas_call(
        functools.partial(halo_kernel, count),
        out_shape=outs,
        in_specs=[VMEM] * 3,
        out_specs=[VMEM] * 3,
        scratch_shapes=[pltpu.SemaphoreType.DMA((2 * REACH, 3))] * 3,
        compiler_params=pltpu.CompilerParams(collective_id=0, has_side_effects=True),
        name="halo",
    )(key_rows, value_rows, ids)


def attention_kernel(lambda_ref, q_ref, k_ref, v_ref, own_ref, all_ref, out_ref):
    head = pl.program_id(0)
    query = q_ref[...]
    lane = lax.broadcasted_iota(jnp.int32, query.shape, 1)
    same = own_ref[...] == all_ref[...]
    scale = jnp.asarray(HD ** (-0.5), query.dtype)
    contract = (((1,), (1,)), ((), ()))

    def lifted(keep):
        part = jnp.where(keep, query * scale, jnp.zeros_like(query))
        scores = lax.dot_general(part, k_ref[...], contract, preferred_element_type=jnp.float32)
        masked = jnp.where(same, scores, -1e30)
        powers = jnp.exp(masked - jnp.max(masked, axis=-1, keepdims=True))
        return powers, jnp.sum(powers, axis=-1, keepdims=True)

    first, first_sum = lifted(lane < HD)
    second, second_sum = lifted(lane >= HD)
    weights = first * (1.0 / first_sum) - second * (lambda_ref[head] / second_sum)
    head_out = jnp.dot(
        weights.astype(jnp.bfloat16), v_ref[...], preferred_element_type=jnp.float32
    )
    scaled = head_out * lax.rsqrt(jnp.mean(head_out * head_out, axis=-1, keepdims=True) + 1e-06)
    out_ref[...] = scaled.astype(jnp.bfloat16)


def attention(query_rows, all_keys, all_values, own_ids, all_ids, mix_lambda):
    length, width = query_rows.shape
    heads = mix_lambda.shape[0]
    wide, keys = width // heads, all_keys.shape[0]
    value_dim = all_values.shape[1] // heads
    rows = min(length, 128)
    return pl.pallas_call(
        attention_kernel,
        grid=(heads, length // rows),
        out_shape=jax.ShapeDtypeStruct((length, heads * value_dim), jnp.bfloat16),
        in_specs=[
            pl.BlockSpec(memory_space=pltpu.SMEM),
            pl.BlockSpec((rows, wide), lambda h, r: (r, h)),
            pl.BlockSpec((keys, wide), lambda h, r: (0, h)),
            pl.BlockSpec((keys, value_dim), lambda h, r: (0, h)),
            pl.BlockSpec((rows, 1), lambda h, r: (r, 0)),
            pl.BlockSpec((1, keys), lambda h, r: (0, 0)),
        ],
        out_specs=pl.BlockSpec((rows, value_dim), lambda h, r: (r, h)),
        name="attention",
    )(mix_lambda, query_rows, all_keys, all_values, own_ids, all_ids)


def greet_all(count, me, core):
    barrier = pltpu.get_barrier_semaphore()
    pl.semaphore_signal(barrier, inc=1, device_id=(me, 1 - core), device_id_type=MESH)

    @pl.loop(1, count)
    def _(step):
        pl.semaphore_signal(
            barrier, inc=1, device_id=((me + step) % count, core), device_id_type=MESH
        )

    pl.semaphore_wait(barrier, count)


def experts_kernel(
    count,
    out_ref,
    gate_hbm,
    up_hbm,
    down_hbm,
    back_ref,
    rows_ref,
    part_ref,
    far_ref,
    sum_ref,
    hidden_ref,
    gate_ref,
    up_ref,
    down_ref,
    load_sem,
    own_sem,
    send_sem,
    recv_sem,
    pass_sem,
    come_sem,
    swap_sem,
    half_sem,
    give_sem,
    take_sem,
):
    me, core = lax.axis_index("sp"), lax.axis_index("tp")
    per = rows_ref.shape[2]
    groups = count // per
    layer, place = me // per, me % per
    greet_all(count, me, core)

    def ahead(g, j):
        return (layer + g) % groups * per + (place + j) % per

    def behind(g, j):
        return (layer - g + groups) % groups * per + (place - j + per) % per

    def remote(source, target, sent, came, at, side):
        return pltpu.make_async_remote_copy(
            src_ref=source,
            dst_ref=target,
            send_sem=sent,
            recv_sem=came,
            device_id=(at, side),
            device_id_type=MESH,
        )

    def across(g, j):
        at = ahead(g, j)
        return remote(
            out_ref.at[at], rows_ref.at[g, core, j], send_sem.at[g, j], recv_sem.at[g, j], at, core
        )

    def forward(g, j, side):
        block = rows_ref.at[g, side, j]
        return remote(block, block, pass_sem.at[g, j], come_sem.at[g, j], me, 1 - core)

    def swap(g):
        return remote(
            part_ref.at[g, 1 - core], far_ref.at[g], swap_sem.at[g], half_sem.at[g], me, 1 - core
        )

    def home(g, j):
        at = behind(g, j)
        return remote(
            sum_ref.at[g, j], back_ref.at[me], give_sem.at[g, j], take_sem.at[g, j], at, core
        )

    def came_home(g, j):
        at = ahead(g, j)
        return remote(
            sum_ref.at[g, j], back_ref.at[at], give_sem.at[g, j], take_sem.at[g, j], at, core
        )

    own = pltpu.make_async_copy(out_ref.at[me], rows_ref.at[0, core, 0], own_sem)
    own.start()

    @pl.loop(1, count)
    def _(step):
        across(step // per, step % per).start()

    loads = [
        pltpu.make_async_copy(source, target, load_sem.at[which])
        for which, (source, target) in enumerate(
            ((gate_hbm, gate_ref), (up_hbm, up_ref), (down_hbm, down_ref))
        )
    ]
    for load in loads:
        load.start()
    own.wait()
    forward(0, 0, core).start()

    @pl.loop(0, groups)
    def _(g):
        for j in range(per):

            @pl.when(g + j > 0)
            def _():
                across(g, j).wait_recv()
                forward(g, j, core).start()

        for j in range(per):
            forward(g, j, 1 - core).wait_recv()

        @pl.when(g == 0)
        def _():
            for load in loads:
                load.wait()

        rows, width = hidden_ref.shape
        model = down_ref.shape[1]
        wide = min(256, width)

        @pl.loop(0, width // wide)
        def _(c):
            cut = pl.ds(pl.multiple_of(c * wide, wide), wide)
            taken = rows_ref[g].reshape(rows, model)
            gate = jnp.dot(taken, gate_ref[:, cut], preferred_element_type=jnp.float32)
            upward = jnp.dot(taken, up_ref[:, cut], preferred_element_type=jnp.float32)
            hidden_ref[:, cut] = (gate / (1.0 + jnp.exp(-gate)) * upward).astype(hidden_ref.dtype)

        @pl.loop(0, model // wide)
        def _(c):
            cut = pl.ds(pl.multiple_of(c * wide, wide), wide)
            product = jnp.dot(
                hidden_ref[...], down_ref[:, cut], preferred_element_type=jnp.float32
            ).astype(part_ref.dtype)
            part_ref[g, :, :, :, cut] = product.reshape(part_ref.shape[1:4] + (wide,))

        swap(g).start()
        swap(g).wait_recv()
        for j in range(per):
            mine = part_ref[g, core, j].astype(jnp.float32)
            sum_ref[g, j] = (mine + far_ref[g, j].astype(jnp.float32)).astype(sum_ref.dtype)
            if j > 0:

                @pl.when(g + j > 1)
                def _():
                    home(g, j - 1).start()

        home(g, per - 1).start()

    back_ref[me] = sum_ref[0, 0]

    @pl.loop(1, count)
    def _(step):
        g, j = step // per, step % per
        came_home(g, j).wait_recv()
        home(g, j).wait_send()
        across(g, j).wait_send()

    @pl.loop(0, count)
    def _(step):
        forward(step // per, step % per, core).wait_send()

    @pl.loop(0, groups)
    def _(g):
        swap(g).wait_send()


def run_experts(count, outgoing, gate_weight, up_weight, down_weight):
    _, capacity, model = outgoing.shape
    per = REACH + 1
    groups = count // per
    hidden = gate_weight.shape[1]
    kept = outgoing.dtype
    each = pltpu.SemaphoreType.DMA((groups, per))
    whole = pltpu.SemaphoreType.DMA((groups,))
    anywhere = pl.BlockSpec(memory_space=pl.ANY)
    return pl.pallas_call(
        functools.partial(experts_kernel, count),
        out_shape=jax.ShapeDtypeStruct(outgoing.shape, kept),
        in_specs=[VMEM, anywhere, anywhere, anywhere],
        out_specs=VMEM,
        scratch_shapes=[
            pltpu.VMEM((groups, 2, per, capacity, model), kept),
            pltpu.VMEM((groups, 2, per, capacity, model), kept),
            pltpu.VMEM((groups, per, capacity, model), kept),
            pltpu.VMEM((groups, per, capacity, model), kept),
            pltpu.VMEM((2 * per * capacity, hidden), kept),
            pltpu.VMEM(gate_weight.shape, kept),
            pltpu.VMEM(up_weight.shape, kept),
            pltpu.VMEM(down_weight.shape, kept),
            pltpu.SemaphoreType.DMA((3,)),
            pltpu.SemaphoreType.DMA,
            each,
            each,
            each,
            each,
            whole,
            whole,
            each,
            each,
        ],
        compiler_params=pltpu.CompilerParams(collective_id=1, has_side_effects=True),
        name="experts",
    )(outgoing, gate_weight, up_weight, down_weight)


def slots_of(routes, experts, capacity):
    flat_routes = routes.reshape(-1)
    table = (flat_routes[:, None] == jnp.arange(experts, dtype=jnp.int32)[None, :]).astype(
        jnp.float32
    )
    count = table.shape[0]
    before = jnp.tril(jnp.ones((count, count), jnp.bfloat16), -1)
    earlier = jnp.dot(before, table.astype(jnp.bfloat16), preferred_element_type=jnp.float32)
    rank = jnp.sum(earlier * table, axis=1).astype(jnp.int32)
    return (flat_routes * capacity + rank).reshape(routes.shape)


def on_device(
    residual,
    query_rows,
    key_rows,
    value_rows,
    mix_lambda,
    documents,
    out_weight,
    norm_gain,
    gate_weight,
    up_weight,
    down_weight,
    routes,
    route_weights,
):
    length = query_rows.shape[0]
    model_width = residual.shape[1]
    experts = lax.axis_size("sp")
    capacity = 2 * length // experts
    top_count = routes.shape[1]
    keys, values, ids = halo(experts, key_rows, value_rows, documents.reshape(1, length))
    merged = attention(
        query_rows,
        keys.reshape(-1, keys.shape[-1]),
        values.reshape(-1, values.shape[-1]),
        documents.reshape(length, 1),
        ids.reshape(1, -1),
        mix_lambda,
    )
    token_heads = lax.all_to_all(merged, "tp", split_axis=0, concat_axis=1, tiled=True)
    projected = jnp.dot(token_heads, out_weight, preferred_element_type=jnp.float32)
    mixed = (residual.astype(jnp.float32) + projected).astype(jnp.bfloat16)
    mixed_wide = mixed.astype(jnp.float32)
    normed = (
        mixed_wide
        * lax.rsqrt(jnp.mean(mixed_wide * mixed_wide, axis=-1, keepdims=True) + 1e-06)
        * norm_gain
    ).astype(jnp.bfloat16)
    slots = slots_of(routes, experts, capacity)
    places = jnp.arange(experts * capacity, dtype=jnp.int32)
    spread = jnp.any(slots[None, :, :] == places[:, None, None], axis=-1).astype(jnp.bfloat16)
    outgoing = jnp.dot(spread, normed, preferred_element_type=jnp.float32).astype(jnp.bfloat16)
    returned = run_experts(
        experts,
        outgoing.reshape(experts, capacity, model_width),
        gate_weight[0],
        up_weight[0],
        down_weight[0],
    ).reshape(-1, model_width)
    weighted = 0.0
    for which in range(top_count):
        pick = (slots[:, which][:, None] == places[None, :]).astype(jnp.bfloat16)
        picked = jnp.dot(pick, returned, preferred_element_type=jnp.float32)
        weighted = weighted + picked * route_weights[:, which][:, None]
    return (mixed_wide + weighted).astype(jnp.bfloat16)


def solution(mesh):
    placed = (
        P(("sp", "tp"), None),
        P("sp", "tp"),
        P("sp", "tp"),
        P("sp", "tp"),
        P("tp"),
        P("sp"),
        P(),
        P(),
        P("sp", None, "tp"),
        P("sp", None, "tp"),
        P("sp", "tp", None),
        P(("sp", "tp"), None),
        P(("sp", "tp"), None),
    )
    return jax.shard_map(
        on_device, mesh=mesh, in_specs=placed, out_specs=P(("sp", "tp"), None), check_vma=False
    )
```

profile of v0, /device:TPU:0, one launch (start us, length us, event | category | flops | bytes accessed | tf_op | source)
XLA Modules:
  0.0 201.3 jit_solution(12842373366484577460)
XLA Ops:
  0.0 1.5 copy.31.own_ref
  1.5 58.4 %halo.1 = (bf16[7,256,512]{2,1,0:T(8,128)(2,1)}, bf16[7,256,512]{2,1,0:T(8,128)(2,1)}, s32[7,1,256]{2,1,0:T(1,128)}) custom-call(bf16[256,512]{1,0:T(8,128)(2,1)} %k_ref.1, bf16[256,512]{1,0:T(8,128)(2,1)} %v_ref.1, s32[1,256]{1,0:T(1,128)} %bitcast.39), custom_call_target="tpu_custom_call" | custom-call | tf_op jit(solution)/shard_map/halo/pallas_call | solution.py:140
  59.9 0.0 copy-start.3
  59.9 0.0 copy-start.1
  59.9 11.1 %attention.1 = bf16[256,512]{1,0:T(8,128)(2,1)} custom-call(f32[4]{0:T(128)} %lambda_ref.1, bf16[256,512]{1,0:T(8,128)(2,1)} %q_ref.1, bf16[1792,512]{1,0:T(8,128)(2,1)} %bitcast.33, bf16[1792,512]{1,0:T(8,128)(2,1)} %bitcast.34, s32[256,1]{1,0:T(8,128)} %copy.31.own_ref, s32[1,1792]{1,0:T(1,128)} %bitcast.37), custom_call_target="tpu_custom_call" | custom-call | tf_op jit(solution)/shard_map/attention/pallas_call | solution.py:182
  70.9 1.8 copy.32
  72.7 3.4 %all-to-all-start = ((bf16[2,128,512]{1,2,0:T(8,128)(2,1)}), bf16[2,128,512]{1,2,0:T(8,128)(2,1)S(1)}, u32[]{:S(2)}, u32[]{:S(2)}) async-start(bf16[2,128,512]{1,2,0:T(8,128)(2,1)} %copy.32), calls=%async_computation | async-start | bytes 524288 | tf_op jit(solution)/shard_map/all_to_all | solution.py:453
  76.2 0.0 copy-done.3
  76.2 0.1 copy.33
  76.3 0.1 eq.58
  76.4 0.3 fusion.5
  76.7 0.1 convert_element_type.42
  76.9 0.1 copy.34
  76.9 0.1 fusion.8
  77.0 0.7 all-to-all-done
  77.7 0.0 copy-done.1
  77.7 0.0 copy-start.4
  77.7 0.0 copy-start.2
  77.7 3.0 %multiply_reduce_fusion = (f32[128]{0:T(128)S(1)}, f32[128,2048]{1,0:T(8,128)S(1)}) fusion(bf16[128,1024]{0,1:T(8,128)(2,1)S(1)} %bitcast.35, bf16[1024,2048]{1,0:T(8,128)(2,1)} %param.19, bf16[128,2048]{1,0:T(8,128)(2,1)S(1)} %copy-done.1), kind=kOutput, calls=%fused_computation.12 | convolution fusion | flops 538443648 | bytes 6029824 | tf_op jit(solution)/shard_map/dot_general | solution.py:454
  80.8 0.0 copy-done.4
  80.8 0.0 copy-done.2
  80.8 2.1 %convolution_convert_fusion = bf16[512,2048]{1,0:T(8,128)(2,1)} fusion(pred[512,128]{1,0:T(8,128)(4,1)S(1)} %fusion.8, f32[128,2048]{1,0:T(8,128)S(1)} %get-tuple-element.16, f32[2048]{0:T(1024)S(1)} %copy-done.2, f32[128]{0:T(128)S(1)} %add_rsqrt_fusion), kind=kOutput, calls=%fused_computation | convolution fusion | flops 270270464 | bytes 3219968 | tf_op jit(solution)/shard_map/dot_general | solution.py:465
  82.9 114.7 %experts.1 = bf16[16,32,2048]{2,1,0:T(8,128)(2,1)} custom-call(bf16[16,32,2048]{2,1,0:T(8,128)(2,1)} %bitcast.29, bf16[2048,1024]{1,0:T(8,128)(2,1)} %bitcast.30, bf16[2048,1024]{1,0:T(8,128)(2,1)} %bitcast.31, bf16[1024,2048]{1,0:T(8,128)(2,1)} %bitcast.32), custom_call_target="tpu_custom_call" | custom-call | tf_op jit(solution)/shard_map/experts/pallas_call | solution.py:382
  197.6 0.0 copy-start
  197.6 2.2 %convolution_multiply_fusion.1 = f32[128,2048]{1,0:T(8,128)S(1)} fusion(bf16[512,2048]{1,0:T(8,128)(2,1)} %bitcast.27, f32[128]{0:T(128)S(1)} %get-tuple-element.14, s32[128]{0:T(128)S(1)} %get-tuple-element.12), kind=kOutput, calls=%fused_computation.4 | convolution fusion | flops 268763136 | bytes 3146752 | tf_op jit(solution)/shard_map/dot_general | solution.py:476
  199.8 0.0 copy-done
  199.8 1.4 fusion.4
  (6 shorter events, 0.0 us)
Async XLA Ops:
  59.9 16.3 %copy-start.3 = (s32[128,2]{0,1:T(2,128)S(1)}, s32[128,2]{0,1:T(2,128)}, u32[]{:S(2)}) copy-start(s32[128,2]{0,1:T(2,128)} %param.24) | copy-start | bytes 3076
  59.9 17.8 %copy-start.1 = (bf16[128,2048]{1,0:T(8,128)(2,1)S(1)}, bf16[128,2048]{1,0:T(8,128)(2,1)}, u32[]{:S(2)}) copy-start(bf16[128,2048]{1,0:T(8,128)(2,1)} %param.13) | copy-start | bytes 1572868
  72.7 5.0 %all-to-all-start = ((bf16[2,128,512]{1,2,0:T(8,128)(2,1)}), bf16[2,128,512]{1,2,0:T(8,128)(2,1)S(1)}, u32[]{:S(2)}, u32[]{:S(2)}) async-start(bf16[2,128,512]{1,2,0:T(8,128)(2,1)} %copy.32), calls=%async_computation | async-start | bytes 524288 | tf_op jit(solution)/shard_map/all_to_all | solution.py:453
  77.7 3.1 %copy-start.4 = (f32[128,2]{0,1:T(2,128)S(1)}, f32[128,2]{0,1:T(2,128)}, u32[]{:S(2)}) copy-start(f32[128,2]{0,1:T(2,128)} %param.25) | copy-start | bytes 3076
  77.7 3.1 %copy-start.2 = (f32[2048]{0:T(1024)S(1)}, f32[2048]{0:T(1024)}, u32[]{:S(2)}) copy-start(f32[2048]{0:T(1024)} %param.20) | copy-start | bytes 24580
  197.6 2.2 %copy-start = (bf16[16,32,2048]{2,1,0:T(8,128)(2,1)S(1)}, bf16[16,32,2048]{2,1,0:T(8,128)(2,1)}, u32[]{:S(2)}) copy-start(bf16[16,32,2048]{2,1,0:T(8,128)(2,1)} %experts.1) | copy-start | bytes 6291460
where the time goes:
time: 202 us; the launch traced here: 201 us
  Pallas kernels  184 us (91%)
  matrix products  9.05 us (4%)
  local copies, waits for them, and re-layouts  3.73 us (2%)
  starting transfers between devices  3.44 us (2%)
    pallas_call x1, Pallas kernels, run_experts(): pl.pallas_call(functools.partial(experts_kernel, count), out_shape=jax.Sh...  115 us
    pallas_call x1, Pallas kernels, halo(): pl.pallas_call(functools.partial(halo_kernel, count), out_shape=outs, in_...  58.4 us
    pallas_call x1, Pallas kernels, attention(): pl.pallas_call(attention_kernel, grid=(heads, length // rows), out_shape=...  11.1 us
  transfers between devices with their start and end apart: 1, of which 1 were waited for; matrix products, arithmetic and copies ran while one was open for 0% of the time, Pallas kernels for 0%

commit v1 on v0

--- a/solution.py
+++ b/solution.py
@@ -13,187 +13,336 @@
 VMEM = pl.BlockSpec(memory_space=pltpu.VMEM)
 
 
-def offsets_of(reach):
-    return [sign * step for step in range(1, reach + 1) for sign in (1, -1)]
-
-
-def halo_kernel(
-    count, k_ref, v_ref, id_ref, k_out, v_out, id_out, send_sem, recv_sem, pass_sem
+def attend_kernel(
+    groups,
+    lambda_ref,
+    q_ref,
+    k_ref,
+    v_ref,
+    id_ref,
+    residual_ref,
+    gain_ref,
+    proj_hbm,
+    mixed_ref,
+    normed_ref,
+    q_all,
+    k_all,
+    v_all,
+    id_all,
+    out_buf,
+    heads_ref,
+    proj_ref,
+    square_ref,
+    proj_sem,
+    in_send,
+    in_recv,
+    hop_send,
+    hop_recv,
+    out_send,
+    out_recv,
 ):
     me, core = lax.axis_index("sp"), lax.axis_index("tp")
-    offsets = offsets_of(REACH)
-    group = REACH + 1
+    per = REACH + 1
+    g, p = me // per, me % per
+    length, wide = q_all.shape[1:]
+    value_dim = v_all.shape[2]
+    rows = mixed_ref.shape[0]
+    cores = length // rows
+    span = 2 * REACH + 1
     barrier = pltpu.get_barrier_semaphore()
 
-    def inside(offset):
-        return jnp.logical_and(me + offset >= 0, me + offset < count)
-
-    for offset in offsets_of(group):
-
-        @pl.when(inside(offset))
+    for side in range(cores):
+        for j in range(per):
+
+            @pl.when(jnp.logical_or(side != core, j > 0))
+            def _():
+                at = g * per + (p + j) % per
+                pl.semaphore_signal(barrier, inc=1, device_id=(at, side), device_id_type=MESH)
+
+    def beyond(step):
+        return jnp.logical_and(g + step >= 0, g + step < groups)
+
+    for step in (1, -1):
+
+        @pl.when(beyond(step))
         def _():
-            pl.semaphore_signal(barrier, inc=1, device_id=(me + offset, core), device_id_type=MESH)
-
-    pl.semaphore_wait(barrier, jnp.minimum(me, group) + jnp.minimum(count - 1 - me, group))
-
-    place = me % group
-
-    def near(offset):
-        return jnp.logical_and(place + offset >= 0, place + offset < group)
-
-    def opposite(offset):
-        return place + (place + offset + group) % group == group - 1
-
-    def copies(at, offset):
-        slot = REACH - offset
-        return [
-            pltpu.make_async_remote_copy(
-                src_ref=source,
-                dst_ref=target.at[slot],
-                send_sem=send_sem.at[at, which],
-                recv_sem=recv_sem.at[at, which],
-                device_id=(me + offset, core),
-                device_id_type=MESH,
-            )
-            for which, (source, target) in enumerate(
-                ((id_ref, id_out), (k_ref, k_out), (v_ref, v_out))
-            )
-        ]
-
-    def passes(at, offset):
-        hop = group if offset < 0 else -group
-        beyond = offset + hop
-        return [
-            pltpu.make_async_remote_copy(
-                src_ref=part.at[REACH - offset],
-                dst_ref=part.at[REACH - beyond],
-                send_sem=pass_sem.at[at, which],
-                recv_sem=recv_sem.at[offsets.index(beyond), which],
-                device_id=(me + hop, core),
-                device_id_type=MESH,
-            )
-            for which, part in enumerate((id_out, k_out, v_out))
-        ]
-
-    def sends(offset):
-        return jnp.logical_and(inside(offset), jnp.logical_or(near(offset), opposite(offset)))
-
-    def relays(offset):
-        hop = group if offset < 0 else -group
-        aligned = jnp.logical_and(inside(-offset), near(-offset))
-        aligned = jnp.logical_and(aligned, jnp.logical_not(opposite(-offset)))
-        return jnp.logical_and(aligned, inside(hop))
-
-    for at, offset in enumerate(offsets):
-
-        @pl.when(sends(offset))
+            at = me + step * per
+            pl.semaphore_signal(barrier, inc=1, device_id=(at, core), device_id_type=MESH)
+
+    others = cores * per - 1
+    pl.semaphore_wait(barrier, others + jnp.minimum(g, 1) + jnp.minimum(groups - 1 - g, 1))
+
+    def remote(source, target, sent, came, at, side):
+        return pltpu.make_async_remote_copy(
+            src_ref=source,
+            dst_ref=target,
+            send_sem=sent,
+            recv_sem=came,
+            device_id=(at, side),
+            device_id_type=MESH,
+        )
+
+    def head_cut(head, width):
+        return pl.ds(pl.multiple_of(head * width, width), width)
+
+    def id_cut(slot):
+        return pl.ds(pl.multiple_of(slot * length, length), length)
+
+    def own_part(which, head):
+        return (
+            id_ref,
+            k_ref.at[:, head_cut(head, wide)],
+            v_ref.at[:, head_cut(head, value_dim)],
+            q_ref.at[:, head_cut(head, wide)],
+        )[which]
+
+    def place_of(which, slot):
+        return (
+            id_all.at[:, id_cut(slot)],
+            k_all.at[slot],
+            v_all.at[slot],
+            q_all.at[slot - REACH],
+        )[which]
+
+    def scatter(j, which):
+        to = (p + j) % per
+        return remote(
+            own_part(which, to),
+            place_of(which, REACH + p),
+            in_send.at[j - 1, which],
+            in_recv.at[j - 1, which],
+            g * per + to,
+            core,
+        )
+
+    def scattered(j, which):
+        source = (p + per - j) % per
+        return remote(
+            own_part(which, source),
+            place_of(which, REACH + source),
+            in_send.at[j - 1, which],
+            in_recv.at[j - 1, which],
+            g * per + source,
+            core,
+        )
+
+    def hop(step, q, which, own):
+        at = 0 if step > 0 else 1
+        source = own_part(which, p) if own else place_of(which, REACH + q)
+        return remote(
+            source,
+            place_of(which, REACH + q - step * per),
+            hop_send.at[at, q, which],
+            hop_recv.at[at, q, which],
+            me + step * per,
+            core,
+        )
+
+    def hopped(step, q, which):
+        at = 0 if step > 0 else 1
+        return remote(
+            own_part(which, p),
+            place_of(which, REACH + q - step * per),
+            hop_send.at[at, q, which],
+            hop_recv.at[at, q, which],
+            me - step * per,
+            core,
+        )
+
+    def hops(step, q):
+        return jnp.logical_and(beyond(step), q > 0 if step > 0 else q < REACH)
+
+    for which in range(4):
+        for j in range(1, per):
+            scatter(j, which).start()
+        if which < 3:
+            for step in (1, -1):
+
+                @pl.when(hops(step, p))
+                def _():
+                    hop(step, p, which, True).start()
+
+    load = pltpu.make_async_copy(proj_hbm, proj_ref, proj_sem)
+    load.start()
+    k_all[REACH + p] = k_ref[:, head_cut(p, wide)]
+    v_all[REACH + p] = v_ref[:, head_cut(p, value_dim)]
+    q_all[p] = q_ref[:, head_cut(p, wide)]
+    id_all[:, id_cut(REACH + p)] = id_ref[...]
+    for step in (1, -1):
+
+        @pl.when(jnp.logical_not(beyond(-step)))
         def _():
-            for copy in copies(at, offset):
-                copy.start()
-
-    k_out[REACH] = k_ref[...]
-    v_out[REACH] = v_ref[...]
-    id_out[REACH] = id_ref[...]
-    for offset in offsets:
-
-        @pl.when(jnp.logical_not(inside(-offset)))
+            for slot in range(REACH):
+                at = slot if step > 0 else span + slot
+                k_all[at] = jnp.zeros_like(k_all[at])
+                v_all[at] = jnp.zeros_like(v_all[at])
+                id_all[:, at * length : (at + 1) * length] = jnp.full(
+                    (1, length), -1, id_all.dtype
+                )
+
+    for which in range(3):
+        for j in range(1, per):
+            scattered(j, which).wait_recv()
+            q = (p + per - j) % per
+            for step in (1, -1):
+
+                @pl.when(hops(step, q))
+                def _():
+                    hop(step, q, which, False).start()
+
+    for j in range(1, per):
+        scattered(j, 3).wait_recv()
+    for which in range(3):
+        for q in range(per):
+            for step in (1, -1):
+                if 0 <= REACH + q - step * per < span + REACH:
+
+                    @pl.when(beyond(-step))
+                    def _():
+                        hopped(step, q, which).wait_recv()
+
+    scale = jnp.asarray(HD ** (-0.5), q_all.dtype)
+    contract = (((1,), (1,)), ((), ()))
+    head = core * per + p
+
+    def give(it):
+        i, half = (p + 1 + it // cores) % per, (core + 1 + it) % cores
+        return remote(
+            out_buf.at[it],
+            heads_ref.at[:, head_cut(head, value_dim)],
+            out_send.at[it],
+            out_recv.at[head],
+            g * per + i,
+            half,
+        )
+
+    def taken(source):
+        return remote(
+            out_buf.at[0],
+            heads_ref.at[:, head_cut(source, value_dim)],
+            out_send.at[0],
+            out_recv.at[source],
+            g * per + source % per,
+            source // per,
+        )
+
+    @pl.loop(0, cores * per)
+    def _(it):
+        i, half = (p + 1 + it // cores) % per, (core + 1 + it) % cores
+        first_row = pl.multiple_of(half * rows, rows)
+        query = q_all[i, pl.ds(first_row, rows), :]
+        lane = lax.broadcasted_iota(jnp.int32, query.shape, 1)
+        own = id_all[:, pl.ds(pl.multiple_of((REACH + i) * length + half * rows, rows), rows)]
+        own = jnp.transpose(jnp.broadcast_to(own, (128, rows)))[:, :1]
+        ids = id_all[:, pl.ds(pl.multiple_of(i * length, length), span * length)]
+        same = own == ids
+        keys = k_all[pl.ds(i, span)].reshape(span * length, wide)
+        values = v_all[pl.ds(i, span)].reshape(span * length, value_dim)
+
+        def lifted(keep):
+            part = jnp.where(keep, query * scale, jnp.zeros_like(query))
+            scores = lax.dot_general(part, keys, contract, preferred_element_type=jnp.float32)
+            masked = jnp.where(same, scores, -1e30)
+            powers = jnp.exp(masked - jnp.max(masked, axis=-1, keepdims=True))
+            return powers, jnp.sum(powers, axis=-1, keepdims=True)
+
+        first, first_sum = lifted(lane < HD)
+        second, second_sum = lifted(lane >= HD)
+        weights = first * (1.0 / first_sum) - second * (lambda_ref[p] / second_sum)
+        head_out = jnp.dot(
+            weights.astype(jnp.bfloat16), values, preferred_element_type=jnp.float32
+        )
+        scaled = head_out * lax.rsqrt(
+            jnp.mean(head_out * head_out, axis=-1, keepdims=True) + 1e-06
+        )
+        out_buf[it] = scaled.astype(jnp.bfloat16)
+
+        @pl.when(it > 0)
         def _():
-            slot = REACH - offset
-            k_out[slot] = jnp.zeros_like(k_ref)
-            v_out[slot] = jnp.zeros_like(v_ref)
-            id_out[slot] = jnp.full_like(id_ref, -1)
-
+            give(it - 1).start()
+
+    last = cores * per - 1
+    heads_ref[:, head_cut(head, value_dim)] = out_buf[last]
+    load.wait()
+    for source in range(cores * per):
+
+        @pl.when(source != head)
+        def _():
+            taken(source).wait_recv()
+
+    model = mixed_ref.shape[1]
+    chunk = min(256, model)
+    square_ref[...] = jnp.zeros_like(square_ref)
+
+    @pl.loop(0, model // chunk)
+    def _(c):
+        cut = head_cut(c, chunk)
+        projected = jnp.dot(heads_ref[...], proj_ref[:, cut], preferred_element_type=jnp.float32)
+        mixed = (residual_ref[:, cut].astype(jnp.float32) + projected).astype(jnp.bfloat16)
+        mixed_ref[:, cut] = mixed
+        mixed_wide = mixed.astype(jnp.float32)
+        square_ref[...] += jnp.sum(mixed_wide * mixed_wide, axis=-1, keepdims=True)
+
+    factor = lax.rsqrt(square_ref[...] * (1.0 / model) + 1e-06)
+
+    @pl.loop(0, model // chunk)
+    def _(c):
+        cut = head_cut(c, chunk)
+        mixed_wide = mixed_ref[:, cut].astype(jnp.float32)
+        normed_ref[:, cut] = (mixed_wide * factor * gain_ref[:, cut]).astype(jnp.bfloat16)
+
+    for which in range(4):
+        for j in range(1, per):
+            scatter(j, which).wait_send()
     for which in range(3):
-        for at, offset in enumerate(offsets):
-
-            @pl.when(relays(offset))
-            def _():
-                copies(at, offset)[which].wait_recv()
-                passes(at, offset)[which].start()
-
-    for at, offset in enumerate(offsets):
-
-        @pl.when(jnp.logical_and(inside(-offset), jnp.logical_not(relays(offset))))
-        def _():
-            for copy in copies(at, offset):
-                copy.wait_recv()
-
-    for at, offset in enumerate(offsets):
-
-        @pl.when(sends(offset))
-        def _():
-            for copy in copies(at, offset):
-                copy.wait_send()
-
-        @pl.when(relays(offset))
-        def _():
-            for copy in passes(at, offset):
-                copy.wait_send()
-
-
-def halo(count, key_rows, value_rows, ids):
-    slots = 2 * REACH + 1
-    outs = [
-        jax.ShapeDtypeStruct((slots,) + part.shape, part.dtype)
-        for part in (key_rows, value_rows, ids)
-    ]
+        for q in range(per):
+            for step in (1, -1):
+
+                @pl.when(hops(step, q))
+                def _():
+                    hop(step, q, which, False).wait_send()
+
+    for it in range(last):
+        give(it).wait_send()
+
+
+def attend(count, query_rows, key_rows, value_rows, ids, mix_lambda, residual, gain, out_weight):
+    length, width = query_rows.shape
+    per = REACH + 1
+    wide, value_dim = width // per, value_rows.shape[1] // per
+    rows, model = residual.shape
+    blocks = 3 * REACH + 1
+    outs = length // rows * per
+    kept = jnp.bfloat16
+    shape = jax.ShapeDtypeStruct((rows, model), kept)
+    dma = pltpu.SemaphoreType.DMA
+    smem = pl.BlockSpec(memory_space=pltpu.SMEM)
+    anywhere = pl.BlockSpec(memory_space=pl.ANY)
     return pl.pallas_call(
-        functools.partial(halo_kernel, count),
-        out_shape=outs,
-        in_specs=[VMEM] * 3,
-        out_specs=[VMEM] * 3,
-        scratch_shapes=[pltpu.SemaphoreType.DMA((2 * REACH, 3))] * 3,
+        functools.partial(attend_kernel, count // per),
+        out_shape=[shape, shape],
+        in_specs=[smem] + [VMEM] * 6 + [anywhere],
+        out_specs=[VMEM] * 2,
+        scratch_shapes=[
+            pltpu.VMEM((per, length, wide), kept),
+            pltpu.VMEM((blocks, length, wide), kept),
+            pltpu.VMEM((blocks, length, value_dim), kept),
+            pltpu.VMEM((1, blocks * length), jnp.int32),
+            pltpu.VMEM((outs, rows, value_dim), kept),
+            pltpu.VMEM((rows, outs * value_dim), kept),
+            pltpu.VMEM(out_weight.shape, kept),
+            pltpu.VMEM((rows, 1), jnp.float32),
+            dma,
+            dma((per - 1, 4)),
+            dma((per - 1, 4)),
+            dma((2, per, 3)),
+            dma((2, per, 3)),
+            dma((outs,)),
+            dma((outs,)),
+        ],
         compiler_params=pltpu.CompilerParams(collective_id=0, has_side_effects=True),
-        name="halo",
-    )(key_rows, value_rows, ids)
-
-
-def attention_kernel(lambda_ref, q_ref, k_ref, v_ref, own_ref, all_ref, out_ref):
-    head = pl.program_id(0)
-    query = q_ref[...]
-    lane = lax.broadcasted_iota(jnp.int32, query.shape, 1)
-    same = own_ref[...] == all_ref[...]
-    scale = jnp.asarray(HD ** (-0.5), query.dtype)
-    contract = (((1,), (1,)), ((), ()))
-
-    def lifted(keep):
-        part = jnp.where(keep, query * scale, jnp.zeros_like(query))
-        scores = lax.dot_general(part, k_ref[...], contract, preferred_element_type=jnp.float32)
-        masked = jnp.where(same, scores, -1e30)
-        powers = jnp.exp(masked - jnp.max(masked, axis=-1, keepdims=True))
-        return powers, jnp.sum(powers, axis=-1, keepdims=True)
-
-    first, first_sum = lifted(lane < HD)
-    second, second_sum = lifted(lane >= HD)
-    weights = first * (1.0 / first_sum) - second * (lambda_ref[head] / second_sum)
-    head_out = jnp.dot(
-        weights.astype(jnp.bfloat16), v_ref[...], preferred_element_type=jnp.float32
-    )
-    scaled = head_out * lax.rsqrt(jnp.mean(head_out * head_out, axis=-1, keepdims=True) + 1e-06)
-    out_ref[...] = scaled.astype(jnp.bfloat16)
-
-
-def attention(query_rows, all_keys, all_values, own_ids, all_ids, mix_lambda):
-    length, width = query_rows.shape
-    heads = mix_lambda.shape[0]
-    wide, keys = width // heads, all_keys.shape[0]
-    value_dim = all_values.shape[1] // heads
-    rows = min(length, 128)
-    return pl.pallas_call(
-        attention_kernel,
-        grid=(heads, length // rows),
-        out_shape=jax.ShapeDtypeStruct((length, heads * value_dim), jnp.bfloat16),
-        in_specs=[
-            pl.BlockSpec(memory_space=pltpu.SMEM),
-            pl.BlockSpec((rows, wide), lambda h, r: (r, h)),
-            pl.BlockSpec((keys, wide), lambda h, r: (0, h)),
-            pl.BlockSpec((keys, value_dim), lambda h, r: (0, h)),
-            pl.BlockSpec((rows, 1), lambda h, r: (r, 0)),
-            pl.BlockSpec((1, keys), lambda h, r: (0, 0)),
-        ],
-        out_specs=pl.BlockSpec((rows, value_dim), lambda h, r: (r, h)),
-        name="attention",
-    )(mix_lambda, query_rows, all_keys, all_values, own_ids, all_ids)
+        name="attend",
+    )(mix_lambda, query_rows, key_rows, value_rows, ids, residual, gain, out_weight)
 
 
 def greet_all(count, me, core):
@@ -441,24 +590,18 @@
     experts = lax.axis_size("sp")
     capacity = 2 * length // experts
     top_count = routes.shape[1]
-    keys, values, ids = halo(experts, key_rows, value_rows, documents.reshape(1, length))
-    merged = attention(
+    mixed, normed = attend(
+        experts,
         query_rows,
-        keys.reshape(-1, keys.shape[-1]),
-        values.reshape(-1, values.shape[-1]),
-        documents.reshape(length, 1),
-        ids.reshape(1, -1),
+        key_rows,
+        value_rows,
+        documents.reshape(1, length),
         mix_lambda,
+        residual,
+        norm_gain.reshape(1, model_width),
+        out_weight,
     )
-    token_heads = lax.all_to_all(merged, "tp", split_axis=0, concat_axis=1, tiled=True)
-    projected = jnp.dot(token_heads, out_weight, preferred_element_type=jnp.float32)
-    mixed = (residual.astype(jnp.float32) + projected).astype(jnp.bfloat16)
     mixed_wide = mixed.astype(jnp.float32)
-    normed = (
-        mixed_wide
-        * lax.rsqrt(jnp.mean(mixed_wide * mixed_wide, axis=-1, keepdims=True) + 1e-06)
-        * norm_gain
-    ).astype(jnp.bfloat16)
     slots = slots_of(routes, experts, capacity)
     places = jnp.arange(experts * capacity, dtype=jnp.int32)
     spread = jnp.any(slots[None, :, :] == places[:, None, None], axis=-1).astype(jnp.bfloat16)

time: 202 us -> 166 us (0.82)
  Pallas kernels: 184 us -> 158 us
  starting transfers between devices: 3.44 us -> 0 us
  local copies, waits for them, and re-layouts: 3.73 us -> 0.47 us
  matrix products: 9.05 us -> 6.94 us
    pallas_call x2 -> x1, Pallas kernels: 69.4 us -> 33.4 us  [attend(): pl.pallas_call(functools.partial(attend_kernel, count // per), out_shape=...]
    pallas_call x1, Pallas kernels: 115 us -> 124 us  [run_experts(): pl.pallas_call(functools.partial(experts_kernel, count), out_shape=jax.Sh...]
    all_to_all x1 -> x0, starting transfers between devices: 3.44 us -> none  [on_device(): lax.all_to_all(merged, 'tp', split_axis=0, concat_axis=1, tiled=True)]
    dot_general x1 -> x0, matrix products: 3.03 us -> none  [on_device(): jnp.dot(token_heads, out_weight, preferred_element_type=jnp.float32)]
  transfers between devices with their start and end apart: 1 -> 0, of which waited for: 1 -> 0; matrix products, arithmetic and copies ran while one was open for 0% -> 0% of each run, Pallas kernels for 0% -> 0%
where the time goes in v1:
time: 166 us; the launch traced here: 165 us
  Pallas kernels  158 us (95%)
  matrix products  6.94 us (4%)
    pallas_call x1, Pallas kernels, run_experts(): pl.pallas_call(functools.partial(experts_kernel, count), out_shape=jax.Sh...  124 us
    pallas_call x1, Pallas kernels, attend(): pl.pallas_call(functools.partial(attend_kernel, count // per), out_shape=...  33.4 us
    dot_general x2, matrix products, on_device(): picked = jnp.dot(pick, returned, preferred_element_type=jnp.float32)  3.6 us

profile of v1, /device:TPU:0, one launch (start us, length us, event | category | flops | bytes accessed | tf_op | source)
XLA Modules:
  0.0 165.4 jit_solution(14987308394295934714)
XLA Ops:
  0.0 0.0 copy-start.2
  0.0 33.4 %attend.1 = (bf16[128,2048]{1,0:T(8,128)(2,1)}, bf16[128,2048]{1,0:T(8,128)(2,1)}) custom-call(f32[4]{0:T(128)} %lambda_ref.1, bf16[256,512]{1,0:T(8,128)(2,1)} %q_ref.1, bf16[256,512]{1,0:T(8,128)(2,1)} %k_ref.1, bf16[256,512]{1,0:T(8,128)(2,1)} %v_ref.1, s32[1,256]{1,0:T(1,128)} %bitcast.26, bf16[128,2048]{1,0:T(8,128)(2,1)} %residual_ref.1, ...), custom_call_target="tpu_custom_call" | custom-call | tf_op jit(solution)/shard_map/attend/pallas_call | solution.py:321
  33.4 0.0 copy-done.2
  33.4 0.1 copy.25
  33.5 0.1 eq.58
  33.6 0.3 fusion.3
  33.9 0.1 convert_element_type.31
  34.1 0.1 copy.26
  34.1 0.1 fusion.4
  34.2 3.1 %convolution_convert_fusion = bf16[512,2048]{1,0:T(8,128)(2,1)} fusion(pred[512,128]{1,0:T(8,128)(4,1)S(1)} %fusion.4, bf16[128,2048]{1,0:T(8,128)(2,1)} %get-tuple-element.8), kind=kOutput, calls=%fused_computation | convolution fusion | flops 269484032 | bytes 2686976 | tf_op jit(solution)/shard_map/dot_general | solution.py:608
  37.3 0.0 copy-start.3
  37.3 124.4 %experts.1 = bf16[16,32,2048]{2,1,0:T(8,128)(2,1)} custom-call(bf16[16,32,2048]{2,1,0:T(8,128)(2,1)} %bitcast.21, bf16[2048,1024]{1,0:T(8,128)(2,1)} %bitcast.22, bf16[2048,1024]{1,0:T(8,128)(2,1)} %bitcast.23, bf16[1024,2048]{1,0:T(8,128)(2,1)} %bitcast.24), custom_call_target="tpu_custom_call" | custom-call | tf_op jit(solution)/shard_map/experts/pallas_call | solution.py:531
  161.7 0.0 copy-start
  161.7 0.0 copy-start.1
  161.8 0.0 copy-done.3
  161.8 2.2 %convolution_multiply_fusion.1 = f32[128,2048]{1,0:T(8,128)S(1)} fusion(bf16[512,2048]{1,0:T(8,128)(2,1)} %bitcast.19, f32[128]{0:T(128)S(1)} %get-tuple-element.12, s32[128]{0:T(128)S(1)} %get-tuple-element.10), kind=kOutput, calls=%fused_computation.4 | convolution fusion | flops 268763136 | bytes 3146752 | tf_op jit(solution)/shard_map/dot_general | solution.py:619
  164.0 0.0 copy-done
  164.0 0.0 copy-done.1
  164.1 1.4 fusion.2
  (5 shorter events, 0.0 us)
Async XLA Ops:
  0.0 33.4 %copy-start.2 = (s32[128,2]{0,1:T(2,128)S(1)}, s32[128,2]{0,1:T(2,128)}, u32[]{:S(2)}) copy-start(s32[128,2]{0,1:T(2,128)} %param.24) | copy-start | bytes 3076
  37.3 124.5 %copy-start.3 = (f32[128,2]{0,1:T(2,128)S(1)}, f32[128,2]{0,1:T(2,128)}, u32[]{:S(2)}) copy-start(f32[128,2]{0,1:T(2,128)} %param.25) | copy-start | bytes 3076
  161.7 2.3 %copy-start = (bf16[16,32,2048]{2,1,0:T(8,128)(2,1)S(1)}, bf16[16,32,2048]{2,1,0:T(8,128)(2,1)}, u32[]{:S(2)}) copy-start(bf16[16,32,2048]{2,1,0:T(8,128)(2,1)} %experts.1) | copy-start | bytes 6291460
  161.7 2.3 %copy-start.1 = (bf16[128,2048]{1,0:T(8,128)(2,1)S(1)}, bf16[128,2048]{1,0:T(8,128)(2,1)}, u32[]{:S(2)}) copy-start(bf16[128,2048]{1,0:T(8,128)(2,1)} %get-tuple-element.7) | copy-start | bytes 1572868

commit v2 on v1

--- a/solution.py
+++ b/solution.py
@@ -360,12 +360,16 @@
 
 def experts_kernel(
     count,
-    out_ref,
+    normed_ref,
+    slot_ref,
     gate_hbm,
     up_hbm,
     down_hbm,
     back_ref,
+    dense_ref,
+    slots_ref,
     rows_ref,
+    pack_ref,
     part_ref,
     far_ref,
     sum_ref,
@@ -374,9 +378,12 @@
     up_ref,
     down_ref,
     load_sem,
-    own_sem,
-    send_sem,
-    recv_sem,
+    slot_send,
+    slot_recv,
+    line_send,
+    line_recv,
+    flat_send,
+    flat_recv,
     pass_sem,
     come_sem,
     swap_sem,
@@ -385,16 +392,13 @@
     take_sem,
 ):
     me, core = lax.axis_index("sp"), lax.axis_index("tp")
-    per = rows_ref.shape[2]
+    per, capacity, model = rows_ref.shape[2:]
     groups = count // per
-    layer, place = me // per, me % per
+    tokens = dense_ref.shape[1]
+    pieces = line_recv.shape[1]
+    piece = tokens // pieces
+    g, p = me // per, me % per
     greet_all(count, me, core)
-
-    def ahead(g, j):
-        return (layer + g) % groups * per + (place + j) % per
-
-    def behind(g, j):
-        return (layer - g + groups) % groups * per + (place - j + per) % per
 
     def remote(source, target, sent, came, at, side):
         return pltpu.make_async_remote_copy(
@@ -406,39 +410,85 @@
             device_id_type=MESH,
         )
 
-    def across(g, j):
-        at = ahead(g, j)
-        return remote(
-            out_ref.at[at], rows_ref.at[g, core, j], send_sem.at[g, j], recv_sem.at[g, j], at, core
-        )
-
-    def forward(g, j, side):
-        block = rows_ref.at[g, side, j]
-        return remote(block, block, pass_sem.at[g, j], come_sem.at[g, j], me, 1 - core)
-
-    def swap(g):
-        return remote(
-            part_ref.at[g, 1 - core], far_ref.at[g], swap_sem.at[g], half_sem.at[g], me, 1 - core
-        )
-
-    def home(g, j):
-        at = behind(g, j)
-        return remote(
-            sum_ref.at[g, j], back_ref.at[me], give_sem.at[g, j], take_sem.at[g, j], at, core
-        )
-
-    def came_home(g, j):
-        at = ahead(g, j)
-        return remote(
-            sum_ref.at[g, j], back_ref.at[at], give_sem.at[g, j], take_sem.at[g, j], at, core
-        )
-
-    own = pltpu.make_async_copy(out_ref.at[me], rows_ref.at[0, core, 0], own_sem)
-    own.start()
-
-    @pl.loop(1, count)
-    def _(step):
-        across(step // per, step % per).start()
+    def tell(t, source):
+        to = (g + t) % groups
+        return remote(
+            slot_ref, slots_ref.at[source], slot_send.at[t], slot_recv.at[t], to * per + p, core
+        )
+
+    def inside(s):
+        return jnp.logical_and(s >= 0, s < groups)
+
+    def line(step, s, part, own):
+        cut = pl.ds(part * piece, piece)
+        return remote(
+            normed_ref.at[cut] if own else dense_ref.at[s, cut],
+            dense_ref.at[s, cut],
+            line_send.at[(1 - step) // 2, s, part],
+            line_recv.at[s, part],
+            me + step * per,
+            core,
+        )
+
+    def flat(s, j):
+        to = (p + j) % per
+        return remote(
+            pack_ref.at[s, to],
+            rows_ref.at[s, core, p],
+            flat_send.at[s, j],
+            flat_recv.at[s, j],
+            g * per + to,
+            core,
+        )
+
+    def flat_came(s, j):
+        source = (p + per - j) % per
+        return remote(
+            pack_ref.at[s, source],
+            rows_ref.at[s, core, source],
+            flat_send.at[s, j],
+            flat_recv.at[s, j],
+            g * per + source,
+            core,
+        )
+
+    def forward(s, q, side):
+        block = rows_ref.at[s, side, q]
+        return remote(block, block, pass_sem.at[s, q], come_sem.at[s, q], me, 1 - core)
+
+    def swap(s):
+        return remote(
+            part_ref.at[s, 1 - core], far_ref.at[s], swap_sem.at[s], half_sem.at[s], me, 1 - core
+        )
+
+    def home(s, q):
+        return remote(
+            sum_ref.at[s, q],
+            back_ref.at[me],
+            give_sem.at[s, q],
+            take_sem.at[g, p],
+            s * per + q,
+            core,
+        )
+
+    def came_home(s, q):
+        return remote(
+            sum_ref.at[s, q],
+            back_ref.at[s * per + q],
+            give_sem.at[s, q],
+            take_sem.at[s, q],
+            s * per + q,
+            core,
+        )
+
+    for t in range(1, groups):
+        tell(t, g).start()
+    for part in range(pieces):
+        for step in (1, -1):
+
+            @pl.when(inside(g + step))
+            def _():
+                line(step, g, part, True).start()
 
     loads = [
         pltpu.make_async_copy(source, target, load_sem.at[which])
@@ -448,34 +498,41 @@
     ]
     for load in loads:
         load.start()
-    own.wait()
-    forward(0, 0, core).start()
-
-    @pl.loop(0, groups)
-    def _(g):
-        for j in range(per):
-
-            @pl.when(g + j > 0)
-            def _():
-                across(g, j).wait_recv()
-                forward(g, j, core).start()
-
-        for j in range(per):
-            forward(g, j, 1 - core).wait_recv()
-
-        @pl.when(g == 0)
-        def _():
-            for load in loads:
-                load.wait()
-
+    dense_ref[g] = normed_ref[...]
+    slots_ref[g] = slot_ref[...]
+
+    lead = 1 - 2 * (2 * g // groups)
+    wide = min(256, model)
+
+    def pack(s):
+        slot = lax.broadcasted_iota(jnp.int32, (per * capacity, tokens), 0) + g * per * capacity
+        table = slots_ref[s]
+        chosen = jnp.logical_or(slot == table[:1], slot == table[1:2])
+        spread = jnp.where(chosen, 1.0, 0.0).astype(dense_ref.dtype)
+
+        @pl.loop(0, model // wide)
+        def _(c):
+            cut = pl.ds(pl.multiple_of(c * wide, wide), wide)
+            taken = jnp.dot(spread, dense_ref[s, :, cut], preferred_element_type=jnp.float32)
+            pack_ref[s, :, :, cut] = taken.astype(pack_ref.dtype).reshape(per, capacity, wide)
+
+        rows_ref[s, core, p] = pack_ref[s, p]
+        for j in range(1, per):
+            flat(s, j).start()
+        forward(s, p, core).start()
+
+    def expert(s):
+        for j in range(1, per):
+            flat_came(s, j).wait_recv()
+            forward(s, (p + per - j) % per, core).start()
+        for q in range(per):
+            forward(s, q, 1 - core).wait_recv()
         rows, width = hidden_ref.shape
-        model = down_ref.shape[1]
-        wide = min(256, width)
 
         @pl.loop(0, width // wide)
         def _(c):
             cut = pl.ds(pl.multiple_of(c * wide, wide), wide)
-            taken = rows_ref[g].reshape(rows, model)
+            taken = rows_ref[s].reshape(rows, model)
             gate = jnp.dot(taken, gate_ref[:, cut], preferred_element_type=jnp.float32)
             upward = jnp.dot(taken, up_ref[:, cut], preferred_element_type=jnp.float32)
             hidden_ref[:, cut] = (gate / (1.0 + jnp.exp(-gate)) * upward).astype(hidden_ref.dtype)
@@ -486,55 +543,113 @@
             product = jnp.dot(
                 hidden_ref[...], down_ref[:, cut], preferred_element_type=jnp.float32
             ).astype(part_ref.dtype)
-            part_ref[g, :, :, :, cut] = product.reshape(part_ref.shape[1:4] + (wide,))
-
-        swap(g).start()
-        swap(g).wait_recv()
-        for j in range(per):
-            mine = part_ref[g, core, j].astype(jnp.float32)
-            sum_ref[g, j] = (mine + far_ref[g, j].astype(jnp.float32)).astype(sum_ref.dtype)
-            if j > 0:
-
-                @pl.when(g + j > 1)
+            part_ref[s, :, :, :, cut] = product.reshape(part_ref.shape[1:4] + (wide,))
+
+        swap(s).start()
+        swap(s).wait_recv()
+
+        def give(q):
+            @pl.when(jnp.logical_or(s != g, q != p))
+            def _():
+                home(s, q).start()
+
+        for q in range(per):
+            mine = part_ref[s, core, q].astype(jnp.float32)
+            sum_ref[s, q] = (mine + far_ref[s, q].astype(jnp.float32)).astype(sum_ref.dtype)
+            if q > 0:
+                give(q - 1)
+        give(per - 1)
+
+    @pl.loop(0, groups + 1)
+    def _(d):
+        @pl.when(d == 1)
+        def _():
+            for t in range(1, groups):
+                tell(t, (g + groups - t) % groups).wait_recv()
+            for load in loads:
+                load.wait()
+
+        def source_of(at, k):
+            s = g + lead * (1 - 2 * k) * at
+            return s, jnp.logical_and(inside(s), jnp.logical_or(at > 0, k == 0))
+
+        for part in range(pieces):
+            for k in range(2):
+                s, valid = source_of(d, k)
+                step = lead * (2 * k - 1)
+
+                @pl.when(jnp.logical_and(valid, d > 0))
                 def _():
-                    home(g, j - 1).start()
-
-        home(g, per - 1).start()
-
-    back_ref[me] = sum_ref[0, 0]
-
-    @pl.loop(1, count)
-    def _(step):
-        g, j = step // per, step % per
-        came_home(g, j).wait_recv()
-        home(g, j).wait_send()
-        across(g, j).wait_send()
-
-    @pl.loop(0, count)
-    def _(step):
-        forward(step // per, step % per, core).wait_send()
+                    line(step, s, part, False).wait_recv()
+
+                    @pl.when(inside(g + step))
+                    def _():
+                        line(step, s, part, False).start()
+
+        @pl.loop(0, 2)
+        def _(k):
+            s, valid = source_of(d, k)
+
+            @pl.when(valid)
+            def _():
+                pack(s)
+
+        @pl.loop(0, 2)
+        def _(k):
+            s, valid = source_of(d - 1, k)
+
+            @pl.when(jnp.logical_and(valid, d > 0))
+            def _():
+                expert(s)
+
+    back_ref[me] = sum_ref[g, p]
 
     @pl.loop(0, groups)
-    def _(g):
-        swap(g).wait_send()
-
-
-def run_experts(count, outgoing, gate_weight, up_weight, down_weight):
-    _, capacity, model = outgoing.shape
+    def _(s):
+        for q in range(per):
+
+            @pl.when(jnp.logical_or(s != g, q != p))
+            def _():
+                came_home(s, q).wait_recv()
+                home(s, q).wait_send()
+
+            forward(s, q, core).wait_send()
+        for j in range(1, per):
+            flat(s, j).wait_send()
+        swap(s).wait_send()
+        for step in (1, -1):
+            sent = s <= g if step > 0 else s >= g
+
+            @pl.when(jnp.logical_and(sent, inside(g + step)))
+            def _():
+                for part in range(pieces):
+                    line(step, s, part, False).wait_send()
+
+    for t in range(1, groups):
+        tell(t, g).wait_send()
+
+
+def run_experts(count, capacity, normed, slots, gate_weight, up_weight, down_weight):
+    tokens, model = normed.shape
     per = REACH + 1
     groups = count // per
     hidden = gate_weight.shape[1]
-    kept = outgoing.dtype
-    each = pltpu.SemaphoreType.DMA((groups, per))
-    whole = pltpu.SemaphoreType.DMA((groups,))
+    kept = normed.dtype
+    pieces = 2
+    dma = pltpu.SemaphoreType.DMA
+    each = dma((groups, per))
+    whole = dma((groups,))
     anywhere = pl.BlockSpec(memory_space=pl.ANY)
     return pl.pallas_call(
         functools.partial(experts_kernel, count),
-        out_shape=jax.ShapeDtypeStruct(outgoing.shape, kept),
-        in_specs=[VMEM, anywhere, anywhere, anywhere],
+        out_shape=jax.ShapeDtypeStruct((count, capacity, model), kept),
+        in_specs=[VMEM, VMEM, anywhere, anywhere, anywhere],
         out_specs=VMEM,
         scratch_shapes=[
+            pltpu.VMEM((groups, tokens, model), kept),
+            pltpu.VMEM((groups,) + slots.shape, jnp.int32),
             pltpu.VMEM((groups, 2, per, capacity, model), kept),
+            pltpu.VMEM((groups, per, capacity, model), kept),
             pltpu.VMEM((groups, 2, per, capacity, model), kept),
             pltpu.VMEM((groups, per, capacity, model), kept),
             pltpu.VMEM((groups, per, capacity, model), kept),
@@ -542,8 +657,11 @@
             pltpu.VMEM(gate_weight.shape, kept),
             pltpu.VMEM(up_weight.shape, kept),
             pltpu.VMEM(down_weight.shape, kept),
-            pltpu.SemaphoreType.DMA((3,)),
-            pltpu.SemaphoreType.DMA,
+            dma((3,)),
+            whole,
+            whole,
+            dma((2, groups, pieces)),
+            dma((groups, pieces)),
             each,
             each,
             each,
@@ -555,7 +673,7 @@
         ],
         compiler_params=pltpu.CompilerParams(collective_id=1, has_side_effects=True),
         name="experts",
-    )(outgoing, gate_weight, up_weight, down_weight)
+    )(normed, slots, gate_weight, up_weight, down_weight)
 
 
 def slots_of(routes, experts, capacity):
@@ -604,14 +722,8 @@
     mixed_wide = mixed.astype(jnp.float32)
     slots = slots_of(routes, experts, capacity)
     places = jnp.arange(experts * capacity, dtype=jnp.int32)
-    spread = jnp.any(slots[None, :, :] == places[:, None, None], axis=-1).astype(jnp.bfloat16)
-    outgoing = jnp.dot(spread, normed, preferred_element_type=jnp.float32).astype(jnp.bfloat16)
     returned = run_experts(
-        experts,
-        outgoing.reshape(experts, capacity, model_width),
-        gate_weight[0],
-        up_weight[0],
-        down_weight[0],
+        experts, capacity, normed, slots.T, gate_weight[0], up_weight[0], down_weight[0]
     ).reshape(-1, model_width)
     weighted = 0.0
     for which in range(top_count):

time: 166 us -> 133 us (0.80)
  the two profiles are of different devices: /device:TPU:0 before, /device:TPU:6 now
where the time goes in v2:
time: 133 us
  Pallas kernels  126 us (95%)
  matrix products  3.86 us (3%)
  local copies, waits for them, and re-layouts  1.92 us (1%)
    pallas_call x1, Pallas kernels, run_experts(): pl.pallas_call(functools.partial(experts_kernel, count), out_shape=jax.Sh...  93.8 us
    pallas_call x1, Pallas kernels, attend(): pl.pallas_call(functools.partial(attend_kernel, count // per), out_shape=...  32.2 us
    dot_general x2, matrix products, on_device(): picked = jnp.dot(pick, returned, preferred_element_type=jnp.float32)  3.59 us

profile of v2, /device:TPU:6, one launch (start us, length us, event | category | flops | bytes accessed | tf_op | source)
XLA Modules:
  0.0 132.6 jit_solution(5380544588391606788)
XLA Ops:
  0.0 0.8 slice_bitcast_fusion
  0.8 0.8 copy.14
  1.5 0.1 eq.45
  1.7 0.3 fusion.3
  2.0 0.1 convert_element_type.25
  2.1 0.1 copy.15
  2.2 0.7 multiply_add_fusion
  2.9 0.0 copy-start.2
  2.9 32.2 %attend.1 = (bf16[128,2048]{1,0:T(8,128)(2,1)}, bf16[128,2048]{1,0:T(8,128)(2,1)}) custom-call(f32[4]{0:T(128)} %lambda_ref.1, bf16[256,512]{1,0:T(8,128)(2,1)} %q_ref.1, bf16[256,512]{1,0:T(8,128)(2,1)} %k_ref.1, bf16[256,512]{1,0:T(8,128)(2,1)} %v_ref.1, s32[1,256]{1,0:T(1,128)} %bitcast.24, bf16[128,2048]{1,0:T(8,128)(2,1)} %residual_ref.1, ...), custom_call_target="tpu_custom_call" | custom-call | tf_op jit(solution)/shard_map/attend/pallas_call | solution.py:321
  35.1 0.0 copy-done.2
  35.1 93.8 %experts.1 = bf16[16,32,2048]{2,1,0:T(8,128)(2,1)} custom-call(bf16[128,2048]{1,0:T(8,128)(2,1)} %get-tuple-element.8.normed_ref, s32[2,128]{1,0:T(2,128)} %bitcast.22, bf16[2048,1024]{1,0:T(8,128)(2,1)} %bitcast.19, bf16[2048,1024]{1,0:T(8,128)(2,1)} %bitcast.20, bf16[1024,2048]{1,0:T(8,128)(2,1)} %bitcast.21), custom_call_target="tpu_custom_call" | custom-call | tf_op jit(solution)/shard_map/experts/pallas_call | solution.py:643
  128.9 0.0 copy-start
  129.0 0.0 copy-start.1
  129.0 2.2 %convolution_multiply_fusion.1 = f32[128,2048]{1,0:T(8,128)S(1)} fusion(bf16[512,2048]{1,0:T(8,128)(2,1)} %bitcast.17, f32[128]{0:T(128)S(1)} %get-tuple-element.12, s32[128]{0:T(128)S(1)} %get-tuple-element.10), kind=kOutput, calls=%fused_computation.3 | convolution fusion | flops 268763136 | bytes 3146752 | tf_op jit(solution)/shard_map/dot_general | solution.py:731
  131.2 0.0 copy-done
  131.2 0.0 copy-done.1
  131.3 1.4 %fusion.2 = bf16[128,2048]{1,0:T(8,128)(2,1)} fusion(f32[128,2048]{1,0:T(8,128)S(1)} %convolution_multiply_fusion.1, bf16[512,2048]{1,0:T(8,128)(2,1)S(1)} %bitcast.18, bf16[128,2048]{1,0:T(8,128)(2,1)S(1)} %copy-done.1, f32[128]{0:T(128)S(1)} %get-tuple-element.11, s32[128]{0:T(128)S(1)} %get-tuple-element.9), kind=kOutput, calls=%fused_computation.4 | convolution fusion | flops 269811712 | bytes 4195328 | tf_op jit(solution)/shard_map/dot_general | solution.py:731
  (3 shorter events, 0.0 us)
Async XLA Ops:
  2.9 32.2 %copy-start.2 = (s32[128,2]{0,1:T(2,128)}, s32[128,2]{0,1:T(2,128)S(1)}, u32[]{:S(2)}) copy-start(s32[128,2]{0,1:T(2,128)S(1)} %multiply_add_fusion) | copy-start | bytes 3076
  128.9 2.3 %copy-start = (bf16[16,32,2048]{2,1,0:T(8,128)(2,1)S(1)}, bf16[16,32,2048]{2,1,0:T(8,128)(2,1)}, u32[]{:S(2)}) copy-start(bf16[16,32,2048]{2,1,0:T(8,128)(2,1)} %experts.1) | copy-start | bytes 6291460
  129.0 2.3 %copy-start.1 = (bf16[128,2048]{1,0:T(8,128)(2,1)S(1)}, bf16[128,2048]{1,0:T(8,128)(2,1)}, u32[]{:S(2)}) copy-start(bf16[128,2048]{1,0:T(8,128)(2,1)} %get-tuple-element.7) | copy-start | bytes 1572868

commit v3 on v2

--- a/solution.py
+++ b/solution.py
@@ -271,7 +271,7 @@
             taken(source).wait_recv()
 
     model = mixed_ref.shape[1]
-    chunk = min(256, model)
+    chunk = min(1024, model)
     square_ref[...] = jnp.zeros_like(square_ref)
 
     @pl.loop(0, model // chunk)
@@ -361,12 +361,16 @@
 def experts_kernel(
     count,
     normed_ref,
-    slot_ref,
+    mixed_ref,
+    routes_ref,
+    share_ref,
     gate_hbm,
     up_hbm,
     down_hbm,
+    out_ref,
     back_ref,
     dense_ref,
+    slot_ref,
     slots_ref,
     rows_ref,
     pack_ref,
@@ -396,8 +400,19 @@
     groups = count // per
     tokens = dense_ref.shape[1]
     pieces = line_recv.shape[1]
-    piece = tokens // pieces
+    halves = half_sem.shape[1]
     g, p = me // per, me % per
+    loads = [
+        pltpu.make_async_copy(source, target, load_sem.at[which])
+        for which, (source, target) in enumerate(
+            ((gate_hbm, gate_ref), (up_hbm, up_ref), (down_hbm, down_ref))
+        )
+    ]
+    for load in loads:
+        load.start()
+    slot_ref[...] = slots_of(routes_ref[...], count, capacity)
+    dense_ref[g] = normed_ref[...]
+    slots_ref[g] = slot_ref[...]
     greet_all(count, me, core)
 
     def remote(source, target, sent, came, at, side):
@@ -419,35 +434,41 @@
     def inside(s):
         return jnp.logical_and(s >= 0, s < groups)
 
+    def part_cut(part, parts):
+        width = model // parts
+        return pl.ds(part * width, width)
+
     def line(step, s, part, own):
-        cut = pl.ds(part * piece, piece)
-        return remote(
-            normed_ref.at[cut] if own else dense_ref.at[s, cut],
-            dense_ref.at[s, cut],
+        cut = part_cut(part, pieces)
+        return remote(
+            normed_ref.at[:, cut] if own else dense_ref.at[s, :, cut],
+            dense_ref.at[s, :, cut],
             line_send.at[(1 - step) // 2, s, part],
             line_recv.at[s, part],
             me + step * per,
             core,
         )
 
-    def flat(s, j):
+    def flat(s, j, part):
         to = (p + j) % per
-        return remote(
-            pack_ref.at[s, to],
-            rows_ref.at[s, core, p],
-            flat_send.at[s, j],
-            flat_recv.at[s, j],
+        cut = part_cut(part, pieces)
+        return remote(
+            pack_ref.at[s, to, :, cut],
+            rows_ref.at[s, core, p, :, cut],
+            flat_send.at[s, j, part],
+            flat_recv.at[s, j, part],
             g * per + to,
             core,
         )
 
-    def flat_came(s, j):
+    def flat_came(s, j, part):
         source = (p + per - j) % per
-        return remote(
-            pack_ref.at[s, source],
-            rows_ref.at[s, core, source],
-            flat_send.at[s, j],
-            flat_recv.at[s, j],
+        cut = part_cut(part, pieces)
+        return remote(
+            pack_ref.at[s, source, :, cut],
+            rows_ref.at[s, core, source, :, cut],
+            flat_send.at[s, j, part],
+            flat_recv.at[s, j, part],
             g * per + source,
             core,
         )
@@ -456,27 +477,35 @@
         block = rows_ref.at[s, side, q]
         return remote(block, block, pass_sem.at[s, q], come_sem.at[s, q], me, 1 - core)
 
-    def swap(s):
-        return remote(
-            part_ref.at[s, 1 - core], far_ref.at[s], swap_sem.at[s], half_sem.at[s], me, 1 - core
-        )
-
-    def home(s, q):
-        return remote(
-            sum_ref.at[s, q],
-            back_ref.at[me],
-            give_sem.at[s, q],
-            take_sem.at[g, p],
+    def swap(s, h):
+        cut = part_cut(h, halves)
+        return remote(
+            part_ref.at[s, 1 - core, :, :, cut],
+            far_ref.at[s, :, :, cut],
+            swap_sem.at[s, h],
+            half_sem.at[s, h],
+            me,
+            1 - core,
+        )
+
+    def home(s, q, h):
+        cut = part_cut(h, halves)
+        return remote(
+            sum_ref.at[s, q, :, cut],
+            back_ref.at[me, :, cut],
+            give_sem.at[s, q, h],
+            take_sem.at[g, p, h],
             s * per + q,
             core,
         )
 
-    def came_home(s, q):
-        return remote(
-            sum_ref.at[s, q],
-            back_ref.at[s * per + q],
-            give_sem.at[s, q],
-            take_sem.at[s, q],
+    def came_home(s, q, h):
+        cut = part_cut(h, halves)
+        return remote(
+            sum_ref.at[s, q, :, cut],
+            back_ref.at[s * per + q, :, cut],
+            give_sem.at[s, q, h],
+            take_sem.at[s, q, h],
             s * per + q,
             core,
         )
@@ -490,40 +519,27 @@
             def _():
                 line(step, g, part, True).start()
 
-    loads = [
-        pltpu.make_async_copy(source, target, load_sem.at[which])
-        for which, (source, target) in enumerate(
-            ((gate_hbm, gate_ref), (up_hbm, up_ref), (down_hbm, down_ref))
-        )
-    ]
-    for load in loads:
-        load.start()
-    dense_ref[g] = normed_ref[...]
-    slots_ref[g] = slot_ref[...]
-
     lead = 1 - 2 * (2 * g // groups)
-    wide = min(256, model)
-
-    def pack(s):
+    wide = min(1024, model)
+
+    def pack(s, part):
         slot = lax.broadcasted_iota(jnp.int32, (per * capacity, tokens), 0) + g * per * capacity
         table = slots_ref[s]
         chosen = jnp.logical_or(slot == table[:1], slot == table[1:2])
         spread = jnp.where(chosen, 1.0, 0.0).astype(dense_ref.dtype)
-
-        @pl.loop(0, model // wide)
-        def _(c):
-            cut = pl.ds(pl.multiple_of(c * wide, wide), wide)
-            taken = jnp.dot(spread, dense_ref[s, :, cut], preferred_element_type=jnp.float32)
-            pack_ref[s, :, :, cut] = taken.astype(pack_ref.dtype).reshape(per, capacity, wide)
-
-        rows_ref[s, core, p] = pack_ref[s, p]
+        cut = part_cut(part, pieces)
+        taken = jnp.dot(spread, dense_ref[s, :, cut], preferred_element_type=jnp.float32)
+        pack_ref[s, :, :, cut] = taken.astype(pack_ref.dtype).reshape(per, capacity, -1)
+        rows_ref[s, core, p, :, cut] = pack_ref[s, p, :, cut]
         for j in range(1, per):
-            flat(s, j).start()
-        forward(s, p, core).start()
+            flat(s, j, part).start()
+        if part == pieces - 1:
+            forward(s, p, core).start()
 
     def expert(s):
         for j in range(1, per):
-            flat_came(s, j).wait_recv()
+            for part in range(pieces):
+                flat_came(s, j, part).wait_recv()
             forward(s, (p + per - j) % per, core).start()
         for q in range(per):
             forward(s, q, 1 - core).wait_recv()
@@ -537,48 +553,51 @@
             upward = jnp.dot(taken, up_ref[:, cut], preferred_element_type=jnp.float32)
             hidden_ref[:, cut] = (gate / (1.0 + jnp.exp(-gate)) * upward).astype(hidden_ref.dtype)
 
-        @pl.loop(0, model // wide)
-        def _(c):
-            cut = pl.ds(pl.multiple_of(c * wide, wide), wide)
-            product = jnp.dot(
-                hidden_ref[...], down_ref[:, cut], preferred_element_type=jnp.float32
-            ).astype(part_ref.dtype)
-            part_ref[s, :, :, :, cut] = product.reshape(part_ref.shape[1:4] + (wide,))
-
-        swap(s).start()
-        swap(s).wait_recv()
-
-        def give(q):
+        for h in range(halves):
+            width = model // halves
+
+            @pl.loop(0, width // wide)
+            def _(c):
+                cut = pl.ds(pl.multiple_of(h * width + c * wide, wide), wide)
+                product = jnp.dot(
+                    hidden_ref[...], down_ref[:, cut], preferred_element_type=jnp.float32
+                ).astype(part_ref.dtype)
+                part_ref[s, :, :, :, cut] = product.reshape(part_ref.shape[1:4] + (wide,))
+
+            swap(s, h).start()
+
+        def give(q, h):
             @pl.when(jnp.logical_or(s != g, q != p))
             def _():
-                home(s, q).start()
-
-        for q in range(per):
-            mine = part_ref[s, core, q].astype(jnp.float32)
-            sum_ref[s, q] = (mine + far_ref[s, q].astype(jnp.float32)).astype(sum_ref.dtype)
-            if q > 0:
-                give(q - 1)
-        give(per - 1)
-
-    @pl.loop(0, groups + 1)
+                home(s, q, h).start()
+
+        for h in range(halves):
+            swap(s, h).wait_recv()
+            cut = part_cut(h, halves)
+            for q in range(per):
+                mine = part_ref[s, core, q, :, cut].astype(jnp.float32)
+                sum_ref[s, q, :, cut] = (mine + far_ref[s, q, :, cut].astype(jnp.float32)).astype(
+                    sum_ref.dtype
+                )
+                if q > 0:
+                    give(q - 1, h)
+            give(per - 1, h)
+
+    for part in range(pieces):
+        pack(g, part)
+    for t in range(1, groups):
+        tell(t, (g + groups - t) % groups).wait_recv()
+    for load in loads:
+        load.wait()
+
+    @pl.loop(1, groups + 1)
     def _(d):
-        @pl.when(d == 1)
-        def _():
-            for t in range(1, groups):
-                tell(t, (g + groups - t) % groups).wait_recv()
-            for load in loads:
-                load.wait()
-
-        def source_of(at, k):
-            s = g + lead * (1 - 2 * k) * at
-            return s, jnp.logical_and(inside(s), jnp.logical_or(at > 0, k == 0))
-
         for part in range(pieces):
             for k in range(2):
-                s, valid = source_of(d, k)
+                s = g + lead * (1 - 2 * k) * d
                 step = lead * (2 * k - 1)
 
-                @pl.when(jnp.logical_and(valid, d > 0))
+                @pl.when(inside(s))
                 def _():
                     line(step, s, part, False).wait_recv()
 
@@ -586,19 +605,19 @@
                     def _():
                         line(step, s, part, False).start()
 
+            @pl.loop(0, 2)
+            def _(k):
+                s = g + lead * (1 - 2 * k) * d
+
+                @pl.when(inside(s))
+                def _():
+                    pack(s, part)
+
         @pl.loop(0, 2)
         def _(k):
-            s, valid = source_of(d, k)
-
-            @pl.when(valid)
-            def _():
-                pack(s)
-
-        @pl.loop(0, 2)
-        def _(k):
-            s, valid = source_of(d - 1, k)
-
-            @pl.when(jnp.logical_and(valid, d > 0))
+            s = g - lead * (d - 1) + k * lead * (2 * d - 1)
+
+            @pl.when(inside(s))
             def _():
                 expert(s)
 
@@ -610,13 +629,45 @@
 
             @pl.when(jnp.logical_or(s != g, q != p))
             def _():
-                came_home(s, q).wait_recv()
-                home(s, q).wait_send()
+                for h in range(halves):
+                    came_home(s, q, h).wait_recv()
+
+    places = lax.broadcasted_iota(jnp.int32, (tokens, count * capacity), 1)
+
+    def upright(row):
+        return jnp.transpose(jnp.broadcast_to(row, (128, tokens)))[:, :1]
+
+    picks = []
+    for k in range(routes_ref.shape[0]):
+        chosen = upright(slot_ref[k : k + 1, :]) == places
+        picks.append(
+            (jnp.where(chosen, 1.0, 0.0).astype(back_ref.dtype), upright(share_ref[k : k + 1, :]))
+        )
+
+    @pl.loop(0, model // wide)
+    def _(c):
+        cut = pl.ds(pl.multiple_of(c * wide, wide), wide)
+        returned = back_ref[:, :, cut].reshape(count * capacity, wide)
+        weighted = 0.0
+        for pick, share in picks:
+            weighted += jnp.dot(pick, returned, preferred_element_type=jnp.float32) * share
+        out_ref[:, cut] = (mixed_ref[:, cut].astype(jnp.float32) + weighted).astype(out_ref.dtype)
+
+    @pl.loop(0, groups)
+    def _(s):
+        for q in range(per):
+
+            @pl.when(jnp.logical_or(s != g, q != p))
+            def _():
+                for h in range(halves):
+                    home(s, q, h).wait_send()
 
             forward(s, q, core).wait_send()
         for j in range(1, per):
-            flat(s, j).wait_send()
-        swap(s).wait_send()
+            for part in range(pieces):
+                flat(s, j, part).wait_send()
+        for h in range(halves):
+            swap(s, h).wait_send()
         for step in (1, -1):
             sent = s <= g if step > 0 else s >= g
 
@@ -629,25 +680,27 @@
         tell(t, g).wait_send()
 
 
-def run_experts(count, capacity, normed, slots, gate_weight, up_weight, down_weight):
+def run_experts(count, capacity, normed, mixed, routes, shares, gate_weight, up_weight, down_weight):
     tokens, model = normed.shape
     per = REACH + 1
     groups = count // per
     hidden = gate_weight.shape[1]
     kept = normed.dtype
-    pieces = 2
+    pieces, halves = 1, 2
     dma = pltpu.SemaphoreType.DMA
     each = dma((groups, per))
     whole = dma((groups,))
     anywhere = pl.BlockSpec(memory_space=pl.ANY)
     return pl.pallas_call(
         functools.partial(experts_kernel, count),
-        out_shape=jax.ShapeDtypeStruct((count, capacity, model), kept),
-        in_specs=[VMEM, VMEM, anywhere, anywhere, anywhere],
+        out_shape=jax.ShapeDtypeStruct((tokens, model), kept),
+        in_specs=[VMEM] * 4 + [anywhere] * 3,
         out_specs=VMEM,
         scratch_shapes=[
+            pltpu.VMEM((count, capacity, model), kept),
             pltpu.VMEM((groups, tokens, model), kept),
-            pltpu.VMEM((groups,) + slots.shape, jnp.int32),
+            pltpu.VMEM(routes.shape, jnp.int32),
+            pltpu.VMEM((groups,) + routes.shape, jnp.int32),
             pltpu.VMEM((groups, 2, per, capacity, model), kept),
             pltpu.VMEM((groups, per, capacity, model), kept),
             pltpu.VMEM((groups, 2, per, capacity, model), kept),
@@ -662,30 +715,34 @@
             whole,
             dma((2, groups, pieces)),
             dma((groups, pieces)),
+            dma((groups, per, pieces)),
+            dma((groups, per, pieces)),
             each,
             each,
-            each,
-            each,
-            whole,
-            whole,
-            each,
-            each,
+            dma((groups, halves)),
+            dma((groups, halves)),
+            dma((groups, per, halves)),
+            dma((groups, per, halves)),
         ],
         compiler_params=pltpu.CompilerParams(collective_id=1, has_side_effects=True),
         name="experts",
-    )(normed, slots, gate_weight, up_weight, down_weight)
+    )(normed, mixed, routes, shares, gate_weight, up_weight, down_weight)
 
 
 def slots_of(routes, experts, capacity):
-    flat_routes = routes.reshape(-1)
-    table = (flat_routes[:, None] == jnp.arange(experts, dtype=jnp.int32)[None, :]).astype(
-        jnp.float32
-    )
-    count = table.shape[0]
-    before = jnp.tril(jnp.ones((count, count), jnp.bfloat16), -1)
-    earlier = jnp.dot(before, table.astype(jnp.bfloat16), preferred_element_type=jnp.float32)
-    rank = jnp.sum(earlier * table, axis=1).astype(jnp.int32)
-    return (flat_routes * capacity + rank).reshape(routes.shape)
+    tokens = routes.shape[1]
+    expert = lax.broadcasted_iota(jnp.int32, (experts, tokens), 0)
+    earlier = lax.broadcasted_iota(jnp.int32, (tokens, tokens), 0)
+    later = lax.broadcasted_iota(jnp.int32, (tokens, tokens), 1)
+    before = jnp.where(earlier < later, 1.0, 0.0).astype(jnp.bfloat16)
+    taken, slots = 0.0, []
+    for k in range(routes.shape[0]):
+        named = jnp.where(expert == routes[k : k + 1], 1.0, 0.0)
+        ahead = jnp.dot(named.astype(jnp.bfloat16), before, preferred_element_type=jnp.float32)
+        rank = jnp.sum(named * (ahead + taken), axis=0, keepdims=True)
+        taken = taken + jnp.sum(named, axis=1, keepdims=True)
+        slots.append(routes[k : k + 1] * capacity + rank.astype(jnp.int32))
+    return jnp.concatenate(slots, axis=0)
 
 
 def on_device(
@@ -707,7 +764,6 @@
     model_width = residual.shape[1]
     experts = lax.axis_size("sp")
     capacity = 2 * length // experts
-    top_count = routes.shape[1]
     mixed, normed = attend(
         experts,
         query_rows,
@@ -719,18 +775,17 @@
         norm_gain.reshape(1, model_width),
         out_weight,
     )
-    mixed_wide = mixed.astype(jnp.float32)
-    slots = slots_of(routes, experts, capacity)
-    places = jnp.arange(experts * capacity, dtype=jnp.int32)
-    returned = run_experts(
-        experts, capacity, normed, slots.T, gate_weight[0], up_weight[0], down_weight[0]
-    ).reshape(-1, model_width)
-    weighted = 0.0
-    for which in range(top_count):
-        pick = (slots[:, which][:, None] == places[None, :]).astype(jnp.bfloat16)
-        picked = jnp.dot(pick, returned, preferred_element_type=jnp.float32)
-        weighted = weighted + picked * route_weights[:, which][:, None]
-    return (mixed_wide + weighted).astype(jnp.bfloat16)
+    return run_experts(
+        experts,
+        capacity,
+        normed,
+        mixed,
+        routes.T,
+        route_weights.T,
+        gate_weight[0],
+        up_weight[0],
+        down_weight[0],
+    )
 
 
 def solution(mesh):

time: 133 us -> 125 us (0.940)
  Pallas kernels: 126 us -> 122 us
  matrix products: 3.86 us -> 0 us
    dot_general x3 -> x0, matrix products: 3.86 us -> none  [the longest x2 3.59 us: on_device(): picked = jnp.dot(pick, returned, preferred_element_type=jnp.float32)]
    pallas_call x1, Pallas kernels: 32.2 us -> 30.2 us  [attend(): pl.pallas_call(functools.partial(attend_kernel, count // per), out_shape=...]
    pallas_call x1, Pallas kernels: 93.8 us -> 92.2 us  [run_experts(): pl.pallas_call(functools.partial(experts_kernel, count), out_shape=jax.Sh...]
where the time goes in v3:
time: 125 us; the launch traced here: 124 us
  Pallas kernels  122 us (98%)
  local copies, waits for them, and re-layouts  1.88 us (2%)
    pallas_call x1, Pallas kernels, run_experts(): pl.pallas_call(functools.partial(experts_kernel, count), out_shape=jax.Sh...  92.2 us
    pallas_call x1, Pallas kernels, attend(): pl.pallas_call(functools.partial(attend_kernel, count // per), out_shape=...  30.2 us

profile of v3, /device:TPU:6, one launch (start us, length us, event | category | flops | bytes accessed | tf_op | source)
XLA Modules:
  0.0 124.4 jit_solution(5624155034158968)
XLA Ops:
  0.0 30.2 %attend.1 = (bf16[128,2048]{1,0:T(8,128)(2,1)}, bf16[128,2048]{1,0:T(8,128)(2,1)}) custom-call(f32[4]{0:T(128)} %lambda_ref.1, bf16[256,512]{1,0:T(8,128)(2,1)} %q_ref.1, bf16[256,512]{1,0:T(8,128)(2,1)} %k_ref.1, bf16[256,512]{1,0:T(8,128)(2,1)} %v_ref.1, s32[1,256]{1,0:T(1,128)} %bitcast.11, bf16[128,2048]{1,0:T(8,128)(2,1)} %residual_ref.1, ...), custom_call_target="tpu_custom_call" | custom-call | tf_op jit(solution)/shard_map/attend/pallas_call | solution.py:321
  30.3 92.2 %experts.1 = bf16[128,2048]{1,0:T(8,128)(2,1)} custom-call(bf16[128,2048]{1,0:T(8,128)(2,1)} %get-tuple-element.7.normed_ref, bf16[128,2048]{1,0:T(8,128)(2,1)} %get-tuple-element.8.mixed_ref, s32[2,128]{1,0:T(2,128)} %bitcast.12, f32[2,128]{1,0:T(2,128)} %bitcast.13, bf16[2048,1024]{1,0:T(8,128)(2,1)} %bitcast.7, bf16[2048,1024]{1,0:T(8,128)(2,1)} %bitcast.8, ...), custom_call_target="tpu_custom_call" | custom-call | tf_op jit(solution)/shard_map/experts/pallas_call | solution.py:694
  122.5 1.9 %copy.15 = bf16[128,2048]{1,0:T(8,128)(2,1)} copy(bf16[128,2048]{1,0:T(8,128)(2,1)} %experts.1) | data formatting | bytes 1048576
